TPU v7x, 32 devices: a whole 2x2x4 slice. The times are simulated.
32 devices in a mesh: sp: 16 (over z, y, x), tp: 2 (over core).
Axes of the slice: x: 2, y: 2, z: 4, core: 2. Of those that a mesh axis runs over, the one named last changes fastest.
Arguments:
- stream_in: bfloat16 [4096, 2048], P('sp'), may hold values from -6 to 6
- norm_gain: float32 [2, 2048], replicated, may hold values from 0.1 to 1.9
- value_weight: bfloat16 [2, 2048, 2048], P(None, 'sp', 'tp'), may hold values from -0.125 to 0.125
- gate_weight: bfloat16 [2, 2048, 2048], P(None, 'sp', 'tp'), may hold values from -0.125 to 0.125
- conv_taps: float32 [2, 31, 2048], P(None, None, 'tp'), may hold values from -5 to 5
- channel_gain: float32 [2, 2048], P(None, 'tp'), may hold values from 0.1 to 1.9
- out_weight: bfloat16 [2, 2048, 2048], P(None, 'tp', 'sp'), may hold values from -0.125 to 0.125
Outputs:
- stream_out: bfloat16 [4096, 2048], P('sp')
All inputs are finite; a program needn't handle non-finite values.
Results may differ from a plain program's by a relative error of at most 0.015.
Values may be sent and summed in bfloat16 or wider, within the bound.
A program may use at most 64 MiB of HBM per device.

v0:
```python
import jax
import jax.numpy as jnp
from jax import lax
from jax.sharding import PartitionSpec as P

LAYERS = 2
epsilon = 1e-05


def passed_along(value, axis, steps):
    count = lax.axis_size(axis)
    leading, last = (max(0, -steps), min(count, count - steps))
    return lax.ppermute(value, axis, [(source, source + steps) for source in range(leading, last)])


def body(stream_in, norm_gain, value_weight, gate_weight, conv_taps, channel_gain, out_weight):
    stream = stream_in
    tok_rows = stream_in.shape[0]
    width = stream_in.shape[1]
    kernel = conv_taps.shape[1]
    local_cols = value_weight.shape[2]
    for layer in range(LAYERS):
        wide = stream.astype(jnp.float32)
        normed = (
            wide
            * lax.rsqrt(jnp.mean(wide * wide, axis=1, keepdims=True) + epsilon)
            * norm_gain[layer]
        ).astype(jnp.bfloat16)
        value = jnp.dot(
            normed,
            lax.all_gather(value_weight[layer], "sp", axis=0, tiled=True),
            preferred_element_type=jnp.float32,
        )
        gate = jnp.dot(
            normed,
            lax.all_gather(gate_weight[layer], "sp", axis=0, tiled=True),
            preferred_element_type=jnp.float32,
        )
        gated = (value * jax.nn.sigmoid(gate)).astype(jnp.bfloat16)
        earlier = passed_along(gated[tok_rows - (kernel - 1) :], "sp", 1)
        padded = jnp.concatenate([earlier, gated], axis=0).astype(jnp.float32)
        taps = conv_taps[layer]
        filtered = jnp.zeros((tok_rows, local_cols), jnp.float32)
        for tap in range(kernel):
            filtered = filtered + taps[tap] * padded[tap : tap + tok_rows]
        sum_first, sum_second = lax.psum(
            (jnp.sum(filtered, axis=1), jnp.sum(filtered * filtered, axis=1)), "tp"
        )
        mean_value = (sum_first / width)[:, None]
        variance = (sum_second / width)[:, None] - mean_value * mean_value
        activated = jax.nn.silu(
            (filtered - mean_value) * lax.rsqrt(variance + epsilon) * channel_gain[layer]
        ).astype(jnp.bfloat16)
        whole_out = lax.all_gather(out_weight[layer], "sp", axis=1, tiled=True)
        terms = jnp.dot(activated, whole_out, preferred_element_type=jnp.float32)
        summed = lax.psum(terms.astype(jnp.bfloat16), "tp").astype(jnp.float32)
        stream = (wide + summed).astype(jnp.bfloat16)
    return stream


def solution(mesh):
    return jax.shard_map(
        body,
        mesh=mesh,
        in_specs=(
            P("sp", None),
            P(),
            P(None, "sp", "tp"),
            P(None, "sp", "tp"),
            P(None, None, "tp"),
            P(None, "tp"),
            P(None, "tp", "sp"),
        ),
        out_specs=P("sp", None),
        check_vma=False,
    )
```

profile of v0, /device:TPU:0, one launch (start us, length us, event | category | flops | bytes accessed | tf_op | source)
XLA Modules:
  0.0 556.1 jit_solution(6253315192449355150)
XLA Ops:
  6.5 2.0 fusion.142
  8.5 0.0 all-gather.15.cloned.1.call-update
  8.6 0.0 all-gather.13.cloned.1.call-start
  8.6 1.9 fusion.141
  10.5 0.0 all-gather.13.cloned.1.call-update
  10.6 0.0 all-gather.17.cloned.1.call-start
  10.6 0.8 fusion.143
  11.4 0.0 all-gather.17.cloned.1.call-update
  11.5 0.0 all-reduce.5.cloned.1.call-start
  11.5 0.3 fusion.18
  11.9 0.1 fusion.146
  11.9 0.1 fusion.145
  12.0 76.4 %all-gather.15.cloned.1.call-done = bf16[1,2048,1024]{2,1,0:T(8,128)(2,1)} async-done(((bf16[1,128,1024]{2,1,0:T(8,128)(2,1)}), bf16[1,2048,1024]{2,1,0:T(8,128)(2,1)}) %all-gather.15.cloned.1.call-update) | async-done | bytes 4194320 | tf_op jit(solution)/shard_map/all_gather | solution.py:36
  88.5 3.6 fusion.56
  92.1 73.4 %all-gather.13.cloned.1.call-done = bf16[1,2048,1024]{2,1,0:T(8,128)(2,1)} async-done(((bf16[1,128,1024]{2,1,0:T(8,128)(2,1)}), bf16[1,2048,1024]{2,1,0:T(8,128)(2,1)}) %all-gather.13.cloned.1.call-update) | async-done | bytes 4194320 | tf_op jit(solution)/shard_map/all_gather | solution.py:31
  165.4 3.5 fusion.53
  169.0 3.4 collective-permute-start
  172.4 1.9 collective-permute-done
  174.2 0.2 maximum_convert_fusion
  174.4 5.8 %fusion.137 = (f32[256]{0:T(256)S(1)}, f32[256]{0:T(256)S(1)}, f32[256,1024]{1,0:T(8,128)S(1)}) fusion(f32[286,1024]{1,0:T(8,128)S(1)} %maximum_convert_fusion, f32[1024]{0:T(1024)S(1)} %bitcast.146, f32[1024]{0:T(1024)S(1)} %bitcast.147, f32[1024]{0:T(1024)S(1)} %bitcast.148, f32[1024]{0:T(1024)S(1)} %bitcast.149, f32[1024]{0:T(1024)S(1)} %bitcast.150, ...), kind=kLoop, calls=%fused_computation.185 | loop fusion | flops 16776704 | bytes 33683456 | tf_op jit(solution)/shard_map/reduce_sum | solution.py:47
  180.2 2.5 all-reduce.1
  182.7 72.8 %all-gather.17.cloned.1.call-done = bf16[1,1024,2048]{2,1,0:T(8,128)(2,1)} async-done(((bf16[1,1024,128]{2,1,0:T(8,128)(2,1)}), bf16[1,1024,2048]{2,1,0:T(8,128)(2,1)}) %all-gather.17.cloned.1.call-update) | async-done | bytes 4194320 | tf_op jit(solution)/shard_map/all_gather | solution.py:54
  255.5 4.7 fusion.12
  260.2 0.0 all-reduce.5.cloned.1.call-update
  260.2 0.0 all-gather.21.cloned.1.call-start
  260.3 0.5 all-gather.21.cloned.1.call-update
  260.8 0.0 all-gather.19.cloned.1.call-start
  260.9 0.5 all-gather.19.cloned.1.call-update
  261.4 0.0 all-gather.23.cloned.1.call-start
  261.4 0.7 all-gather.23.cloned.1.call-update
  262.1 0.0 all-reduce.7.cloned.1.call-start
  262.2 15.8 %all-reduce.5.cloned.1.call-done = bf16[256,2048]{1,0:T(8,128)(2,1)} async-done(((bf16[256,2048]{1,0:T(8,128)(2,1)}), bf16[256,2048]{1,0:T(8,128)(2,1)}) %all-reduce.5.cloned.1.call-update) | async-done | bytes 1048592 | tf_op jit(solution)/shard_map/psum | solution.py:56
  278.0 1.7 fusion.22
  279.7 77.7 %all-gather.21.cloned.1.call-done = bf16[1,2048,1024]{2,1,0:T(8,128)(2,1)} async-done(((bf16[1,128,1024]{2,1,0:T(8,128)(2,1)}), bf16[1,2048,1024]{2,1,0:T(8,128)(2,1)}) %all-gather.21.cloned.1.call-update) | async-done | bytes 4194320 | tf_op jit(solution)/shard_map/all_gather | solution.py:36
  357.4 3.6 fusion.59
  361.0 73.3 %all-gather.19.cloned.1.call-done = bf16[1,2048,1024]{2,1,0:T(8,128)(2,1)} async-done(((bf16[1,128,1024]{2,1,0:T(8,128)(2,1)}), bf16[1,2048,1024]{2,1,0:T(8,128)(2,1)}) %all-gather.19.cloned.1.call-update) | async-done | bytes 4194320 | tf_op jit(solution)/shard_map/all_gather | solution.py:31
  434.3 3.5 fusion.50
  437.8 3.5 collective-permute-start.1
  441.4 0.1 fusion.144
  441.5 1.6 collective-permute-done.1
  443.1 0.1 maximum_convert_fusion.1
  443.2 5.8 %fusion.136 = (f32[256]{0:T(256)S(1)}, f32[256]{0:T(256)S(1)}, f32[256,1024]{1,0:T(8,128)S(1)}) fusion(f32[286,1024]{1,0:T(8,128)S(1)} %maximum_convert_fusion.1, f32[1024]{0:T(1024)S(1)} %bitcast.112, f32[1024]{0:T(1024)S(1)} %bitcast.113, f32[1024]{0:T(1024)S(1)} %bitcast.156, f32[1024]{0:T(1024)S(1)} %bitcast.157, f32[1024]{0:T(1024)S(1)} %bitcast.158, ...), kind=kLoop, calls=%fused_computation.184 | loop fusion | flops 16776704 | bytes 33683456 | tf_op jit(solution)/shard_map/reduce_sum | solution.py:47
  449.1 2.5 all-reduce
  451.5 72.8 %all-gather.23.cloned.1.call-done = bf16[1,1024,2048]{2,1,0:T(8,128)(2,1)} async-done(((bf16[1,1024,128]{2,1,0:T(8,128)(2,1)}), bf16[1,1024,2048]{2,1,0:T(8,128)(2,1)}) %all-gather.23.cloned.1.call-update) | async-done | bytes 4194320 | tf_op jit(solution)/shard_map/all_gather | solution.py:54
  524.3 4.7 fusion.15
  529.0 0.0 all-reduce.7.cloned.1.call-update
  529.0 17.8 %all-reduce.7.cloned.1.call-done = bf16[256,2048]{1,0:T(8,128)(2,1)} async-done(((bf16[256,2048]{1,0:T(8,128)(2,1)}), bf16[256,2048]{1,0:T(8,128)(2,1)}) %all-reduce.7.cloned.1.call-update) | async-done | bytes 1048592 | tf_op jit(solution)/shard_map/psum | solution.py:56
  546.8 2.5 fusion.25
  (20 shorter events, 0.1 us)
Async XLA Ops:
  6.5 4.1 copy-start.1
  6.5 5.0 copy-start
  6.5 81.9 %all-gather.15.cloned.1.call-start = ((), (), s32[]{:S(2)}) async-start(), calls=%async_computation.3 | async-start | bytes 4456448 | tf_op jit(solution)/shard_map/all_gather | solution.py:36
  8.5 3.3 copy-start.2
  8.5 3.5 copy-start.3
  8.6 156.9 %all-gather.13.cloned.1.call-start = ((), (), s32[]{:S(2)}) async-start(), calls=%async_computation.2 | async-start | bytes 4456448 | tf_op jit(solution)/shard_map/all_gather | solution.py:31
  10.6 244.9 %all-gather.17.cloned.1.call-start = ((), (), s32[]{:S(2)}) async-start(), calls=%async_computation.4 | async-start | bytes 4456448 | tf_op jit(solution)/shard_map/all_gather | solution.py:54
  11.5 266.5 %all-reduce.5.cloned.1.call-start = ((), (), s32[]{:S(2)}) async-start(), calls=%async_computation | async-start | bytes 2097152 | tf_op jit(solution)/shard_map/psum | solution.py:56
  92.0 80.3 %copy-start.4 = (f32[2,1024]{1,0:T(2,128)S(1)}, f32[2,1024]{1,0:T(2,128)}, u32[]{:S(2)}) copy-start(f32[2,1024]{1,0:T(2,128)} %param.12) | copy-start | bytes 24580
  169.0 5.2 collective-permute-start
  260.2 97.2 %all-gather.21.cloned.1.call-start = ((), (), s32[]{:S(2)}) async-start(), calls=%async_computation.6 | async-start | bytes 4456448 | tf_op jit(solution)/shard_map/all_gather | solution.py:36
  260.8 173.5 %all-gather.19.cloned.1.call-start = ((), (), s32[]{:S(2)}) async-start(), calls=%async_computation.5 | async-start | bytes 4456448 | tf_op jit(solution)/shard_map/all_gather | solution.py:31
  261.4 262.9 %all-gather.23.cloned.1.call-start = ((), (), s32[]{:S(2)}) async-start(), calls=%async_computation.7 | async-start | bytes 4456448 | tf_op jit(solution)/shard_map/all_gather | solution.py:54
  262.1 284.6 %all-reduce.7.cloned.1.call-start = ((), (), s32[]{:S(2)}) async-start(), calls=%async_computation.1 | async-start | bytes 2097152 | tf_op jit(solution)/shard_map/psum | solution.py:56
  437.8 5.3 collective-permute-start.1
Sparse Core Ops, SparseCore 0:
  10.1 78.3 all-gather.14
  91.2 74.1 all-gather.12
  168.2 87.3 all-gather.16
  260.3 17.5 all-reduce.4
  280.6 76.7 all-gather.20
  360.0 74.1 all-gather.18
  437.0 87.3 all-gather.22
  529.1 17.5 all-reduce.6
where the time goes:
time: 557 us; the launch traced here: 556 us
  waiting for transfers between devices  485 us (87%)
  matrix products  23.6 us (4%)
  other arithmetic  16.5 us (3%)
  between operations  13.7 us (2%)
  starting transfers between devices  7.18 us (1%)
    all_gather x2, waiting for transfers between devices, body(): lax.all_gather(gate_weight[layer], 'sp', axis=0, tiled=True)  154 us
    all_gather x2, waiting for transfers between devices, body(): lax.all_gather(value_weight[layer], 'sp', axis=0, tiled=True)  147 us
    all_gather x2, waiting for transfers between devices, body(): whole_out = lax.all_gather(out_weight[layer], 'sp', axis=1, tiled=True)  146 us
    psum x2, waiting for transfers between devices, body(): summed = lax.psum(terms.astype(jnp.bfloat16), 'tp').astype(jnp.float32)  33.6 us
    reduce_sum x2, other arithmetic, body(): jnp.sum(filtered, axis=1)  11.6 us
  transfers between devices with their start and end apart: 10, of which 10 were waited for; matrix products, arithmetic and copies ran while one was open for 6% of the time, Pallas kernels for 0%

commit v1 on v0

--- a/solution.py
+++ b/solution.py
@@ -53,7 +53,9 @@
         ).astype(jnp.bfloat16)
         whole_out = lax.all_gather(out_weight[layer], "sp", axis=1, tiled=True)
         terms = jnp.dot(activated, whole_out, preferred_element_type=jnp.float32)
-        summed = lax.psum(terms.astype(jnp.bfloat16), "tp").astype(jnp.float32)
+        summed = jnp.sum(lax.all_gather(terms.astype(jnp.bfloat16), "tp"), axis=0).astype(
+            jnp.float32
+        )
         stream = (wide + summed).astype(jnp.bfloat16)
     return stream
 

time: 557 us -> 540 us (0.969)
  waiting for transfers between devices: 485 us -> 467 us
    psum x2 -> x0, waiting for transfers between devices: 33.6 us -> none  [body(): summed = lax.psum(terms.astype(jnp.bfloat16), 'tp').astype(jnp.float32)]
    all_gather x0 -> x2, waiting for transfers between devices: none -> 15.9 us  [body(): lax.all_gather(terms.astype(jnp.bfloat16), 'tp')]
where the time goes in v1:
time: 540 us; the launch traced here: 539 us
  waiting for transfers between devices  467 us (86%)
  matrix products  23.6 us (4%)
  other arithmetic  18.4 us (3%)
  between operations  13.7 us (3%)
  starting transfers between devices  7.17 us (1%)
    all_gather x2, waiting for transfers between devices, body(): lax.all_gather(gate_weight[layer], 'sp', axis=0, tiled=True)  153 us
    all_gather x2, waiting for transfers between devices, body(): lax.all_gather(value_weight[layer], 'sp', axis=0, tiled=True)  147 us
    all_gather x2, waiting for transfers between devices, body(): whole_out = lax.all_gather(out_weight[layer], 'sp', axis=1, tiled=True)  146 us
    all_gather x2, waiting for transfers between devices, body(): lax.all_gather(terms.astype(jnp.bfloat16), 'tp')  15.9 us
    reduce_sum x2, other arithmetic, body(): jnp.sum(filtered, axis=1)  11.6 us
  transfers between devices with their start and end apart: 10, of which 10 were waited for; matrix products, arithmetic and copies ran while one was open for 6% of the time, Pallas kernels for 0%

profile of v1, /device:TPU:0, one launch (start us, length us, event | category | flops | bytes accessed | tf_op | source)
XLA Modules:
  0.0 539.4 jit_solution(2713619507272308410)
XLA Ops:
  6.5 2.0 fusion.142
  8.6 0.0 all-gather.19.cloned.1.call-update
  8.6 0.0 all-gather.17.cloned.1.call-start
  8.7 1.9 fusion.141
  10.6 0.0 all-gather.17.cloned.1.call-update
  10.6 0.0 all-gather.21.cloned.1.call-start
  10.7 0.8 fusion.143
  11.5 0.0 all-gather.21.cloned.1.call-update
  11.5 0.0 all-gather.23.cloned.1.call-start
  11.6 0.3 fusion.18
  11.9 0.1 fusion.146
  12.0 0.1 fusion.145
  12.1 76.3 %all-gather.19.cloned.1.call-done = bf16[1,2048,1024]{2,1,0:T(8,128)(2,1)} async-done(((bf16[1,128,1024]{2,1,0:T(8,128)(2,1)}), bf16[1,2048,1024]{2,1,0:T(8,128)(2,1)}) %all-gather.19.cloned.1.call-update) | async-done | bytes 4194320 | tf_op jit(solution)/shard_map/all_gather | solution.py:36
  88.5 3.6 fusion.56
  92.1 73.4 %all-gather.17.cloned.1.call-done = bf16[1,2048,1024]{2,1,0:T(8,128)(2,1)} async-done(((bf16[1,128,1024]{2,1,0:T(8,128)(2,1)}), bf16[1,2048,1024]{2,1,0:T(8,128)(2,1)}) %all-gather.17.cloned.1.call-update) | async-done | bytes 4194320 | tf_op jit(solution)/shard_map/all_gather | solution.py:31
  165.4 3.5 fusion.53
  169.0 3.4 collective-permute-start
  172.4 1.9 collective-permute-done
  174.2 0.2 maximum_convert_fusion
  174.4 5.8 %fusion.137 = (f32[256]{0:T(256)S(1)}, f32[256]{0:T(256)S(1)}, f32[256,1024]{1,0:T(8,128)S(1)}) fusion(f32[286,1024]{1,0:T(8,128)S(1)} %maximum_convert_fusion, f32[1024]{0:T(1024)S(1)} %bitcast.150, f32[1024]{0:T(1024)S(1)} %bitcast.151, f32[1024]{0:T(1024)S(1)} %bitcast.152, f32[1024]{0:T(1024)S(1)} %bitcast.153, f32[1024]{0:T(1024)S(1)} %bitcast.154, ...), kind=kLoop, calls=%fused_computation.185 | loop fusion | flops 16776704 | bytes 33683456 | tf_op jit(solution)/shard_map/reduce_sum | solution.py:47
  180.2 2.5 all-reduce.1
  182.7 72.8 %all-gather.21.cloned.1.call-done = bf16[1,1024,2048]{2,1,0:T(8,128)(2,1)} async-done(((bf16[1,1024,128]{2,1,0:T(8,128)(2,1)}), bf16[1,1024,2048]{2,1,0:T(8,128)(2,1)}) %all-gather.21.cloned.1.call-update) | async-done | bytes 4194320 | tf_op jit(solution)/shard_map/all_gather | solution.py:54
  255.5 4.7 fusion.12
  260.2 0.0 all-gather.27.cloned.1.call-start
  260.3 0.5 all-gather.27.cloned.1.call-update
  260.8 0.0 all-gather.25.cloned.1.call-start
  260.9 0.5 all-gather.25.cloned.1.call-update
  261.4 0.0 all-gather.29.cloned.1.call-start
  261.4 0.7 all-gather.29.cloned.1.call-update
  262.1 0.0 all-gather.31.cloned.1.call-start
  262.2 6.9 %all-gather.23.cloned.1.call-done = bf16[512,2048]{1,0:T(8,128)(2,1)} async-done(((bf16[256,2048]{1,0:T(8,128)(2,1)}), bf16[512,2048]{1,0:T(8,128)(2,1)}) %all-gather.23.cloned.1.call-update) | async-done | bytes 2097168 | tf_op jit(solution)/shard_map/all_gather | solution.py:56
  269.1 2.1 reduce_sum.81
  271.3 0.5 fusion.22
  271.8 76.8 %all-gather.27.cloned.1.call-done = bf16[1,2048,1024]{2,1,0:T(8,128)(2,1)} async-done(((bf16[1,128,1024]{2,1,0:T(8,128)(2,1)}), bf16[1,2048,1024]{2,1,0:T(8,128)(2,1)}) %all-gather.27.cloned.1.call-update) | async-done | bytes 4194320 | tf_op jit(solution)/shard_map/all_gather | solution.py:36
  348.5 3.6 fusion.59
  352.1 73.3 %all-gather.25.cloned.1.call-done = bf16[1,2048,1024]{2,1,0:T(8,128)(2,1)} async-done(((bf16[1,128,1024]{2,1,0:T(8,128)(2,1)}), bf16[1,2048,1024]{2,1,0:T(8,128)(2,1)}) %all-gather.25.cloned.1.call-update) | async-done | bytes 4194320 | tf_op jit(solution)/shard_map/all_gather | solution.py:31
  425.4 3.5 fusion.50
  428.9 3.5 collective-permute-start.1
  432.5 0.1 fusion.144
  432.6 1.6 collective-permute-done.1
  434.2 0.1 maximum_convert_fusion.1
  434.3 5.8 %fusion.136 = (f32[256]{0:T(256)S(1)}, f32[256]{0:T(256)S(1)}, f32[256,1024]{1,0:T(8,128)S(1)}) fusion(f32[286,1024]{1,0:T(8,128)S(1)} %maximum_convert_fusion.1, f32[1024]{0:T(1024)S(1)} %bitcast.116, f32[1024]{0:T(1024)S(1)} %bitcast.117, f32[1024]{0:T(1024)S(1)} %bitcast.160, f32[1024]{0:T(1024)S(1)} %bitcast.161, f32[1024]{0:T(1024)S(1)} %bitcast.162, ...), kind=kLoop, calls=%fused_computation.184 | loop fusion | flops 16776704 | bytes 33683456 | tf_op jit(solution)/shard_map/reduce_sum | solution.py:47
  440.2 2.5 all-reduce
  442.7 72.8 %all-gather.29.cloned.1.call-done = bf16[1,1024,2048]{2,1,0:T(8,128)(2,1)} async-done(((bf16[1,1024,128]{2,1,0:T(8,128)(2,1)}), bf16[1,1024,2048]{2,1,0:T(8,128)(2,1)}) %all-gather.29.cloned.1.call-update) | async-done | bytes 4194320 | tf_op jit(solution)/shard_map/all_gather | solution.py:54
  515.4 4.7 fusion.15
  520.1 8.9 %all-gather.31.cloned.1.call-done = bf16[512,2048]{1,0:T(8,128)(2,1)} async-done(((bf16[256,2048]{1,0:T(8,128)(2,1)}), bf16[512,2048]{1,0:T(8,128)(2,1)}) %all-gather.31.cloned.1.call-update) | async-done | bytes 2097168 | tf_op jit(solution)/shard_map/all_gather | solution.py:56
  529.1 2.1 reduce_sum.85
  531.2 1.4 fusion.25
  (22 shorter events, 0.2 us)
Async XLA Ops:
  6.5 4.1 copy-start.1
  6.5 5.0 copy-start
  6.5 81.9 %all-gather.19.cloned.1.call-start = ((), (), s32[]{:S(2)}) async-start(), calls=%async_computation.1 | async-start | bytes 4456448 | tf_op jit(solution)/shard_map/all_gather | solution.py:36
  8.6 3.3 copy-start.2
  8.6 3.5 copy-start.3
  8.6 156.8 %all-gather.17.cloned.1.call-start = ((), (), s32[]{:S(2)}) async-start(), calls=%async_computation | async-start | bytes 4456448 | tf_op jit(solution)/shard_map/all_gather | solution.py:31
  10.6 244.9 %all-gather.21.cloned.1.call-start = ((), (), s32[]{:S(2)}) async-start(), calls=%async_computation.2 | async-start | bytes 4456448 | tf_op jit(solution)/shard_map/all_gather | solution.py:54
  11.5 257.6 %all-gather.23.cloned.1.call-start = ((), (), s32[]{:S(2)}) async-start(), calls=%async_computation.3 | async-start | bytes 3145728 | tf_op jit(solution)/shard_map/all_gather | solution.py:56
  92.0 80.3 %copy-start.4 = (f32[2,1024]{1,0:T(2,128)S(1)}, f32[2,1024]{1,0:T(2,128)}, u32[]{:S(2)}) copy-start(f32[2,1024]{1,0:T(2,128)} %param.12) | copy-start | bytes 24580
  169.0 5.2 collective-permute-start
  260.2 88.3 %all-gather.27.cloned.1.call-start = ((), (), s32[]{:S(2)}) async-start(), calls=%async_computation.5 | async-start | bytes 4456448 | tf_op jit(solution)/shard_map/all_gather | solution.py:36
  260.8 164.6 %all-gather.25.cloned.1.call-start = ((), (), s32[]{:S(2)}) async-start(), calls=%async_computation.4 | async-start | bytes 4456448 | tf_op jit(solution)/shard_map/all_gather | solution.py:31
  261.4 254.0 %all-gather.29.cloned.1.call-start = ((), (), s32[]{:S(2)}) async-start(), calls=%async_computation.6 | async-start | bytes 4456448 | tf_op jit(solution)/shard_map/all_gather | solution.py:54
  262.1 266.9 %all-gather.31.cloned.1.call-start = ((), (), s32[]{:S(2)}) async-start(), calls=%async_computation.7 | async-start | bytes 3145728 | tf_op jit(solution)/shard_map/all_gather | solution.py:56
  428.9 5.2 collective-permute-start.1
Sparse Core Ops, SparseCore 0:
  10.1 78.3 all-gather.18
  91.2 74.1 all-gather.16
  168.2 87.3 all-gather.20
  260.3 8.7 all-gather.22
  271.7 76.7 all-gather.26
  351.2 74.1 all-gather.24
  428.1 87.3 all-gather.28
  520.3 8.7 all-gather.30
